TPU v7x, 128 devices: a whole 4x4x4 slice. The times are simulated.
128 devices in a mesh: fs: 16 (over z, y), tp: 8 (over x, core).
Axes of the slice: x: 4, y: 4, z: 4, core: 2. Of those that a mesh axis runs over, the one named last changes fastest.
Arguments:
- stream: bfloat16 [16384, 1024], P(('fs', 'tp')), may hold values from -3 to 3
- mixer_out: bfloat16 [16384, 1024], P(('fs', 'tp')), may hold values from -6 to 6
- ffn_gains: float32 [4, 1024], replicated, may hold values from 0.5 to 1.5
- mixer_gain: float32 [1024], replicated, may hold values from 0.25 to 0.6
- gate_first: bfloat16 [1024, 2816], P('fs', 'tp'), may hold values from -0.1875 to 0.1875
- up_first: bfloat16 [1024, 2816], P('fs', 'tp'), may hold values from -0.1875 to 0.1875
- down_first: bfloat16 [2816, 1024], P('tp', 'fs'), may hold values from -0.109375 to 0.109375
- gate_second: bfloat16 [1024, 2816], P('fs', 'tp'), may hold values from -0.1875 to 0.1875
- up_second: bfloat16 [1024, 2816], P('fs', 'tp'), may hold values from -0.1875 to 0.1875
- down_second: bfloat16 [2816, 1024], P('tp', 'fs'), may hold values from -0.109375 to 0.109375
Outputs:
- layer_out: bfloat16 [16384, 1024], P(('fs', 'tp'))
All inputs are finite; a program needn't handle non-finite values.
Results may differ from a plain program's by a relative error of at most 0.02.
Values may be sent and summed in bfloat16 or wider, within the bound.
A program may use at most 64 MiB of HBM per device.

v0:
```python
import jax
import jax.numpy as jnp
from jax import lax
from jax.sharding import PartitionSpec as P

epsilon = 1e-06
half_weight = 0.5


def laid_out(blocks, dim):
    dims = list(blocks.shape[1:])
    dims[dim] *= blocks.shape[0]
    return jnp.moveaxis(blocks, 0, dim).reshape(dims)


def gather_together(arrays, axis, dims):
    line = jnp.concatenate([a.reshape(-1) for a in arrays])
    lines, at, gathered = (lax.all_gather(line, axis), 0, [])
    for a, dim in zip(arrays, dims):
        blocks = lines[:, at : at + a.size].reshape(-1, *a.shape)
        gathered.append(laid_out(blocks, dim))
        at += a.size
    return tuple(gathered)


def on_whole(shard, axis, dim, work):
    return work(lax.all_gather(shard, axis, axis=dim, tiled=True), jnp.int32(0))


def own_rows(portion, rows, axis):
    count = rows * lax.axis_size(axis)
    sent = portion(jnp.int32(0), count).astype(jnp.bfloat16)
    return lax.psum_scatter(sent, axis, scatter_dimension=0, tiled=True).astype(jnp.float32)


def rms_rows(values, gain_row):
    widened = values.astype(jnp.float32)
    inverse_rms = lax.rsqrt(jnp.mean(widened * widened, axis=-1, keepdims=True) + epsilon)
    return (widened * inverse_rms * gain_row.astype(jnp.float32)).astype(jnp.bfloat16)


def add_branch(rows, normed_branch, factor):
    return (rows.astype(jnp.float32) + factor * normed_branch.astype(jnp.float32)).astype(
        jnp.bfloat16
    )


def collect_weights(gate_local, up_local, down_local):
    gate_full, up_full = gather_together((gate_local, up_local), "fs", (0, 0))
    down_full = lax.all_gather(down_local, "fs", axis=1, tiled=True)
    return (gate_full, up_full, down_full)


def half_step(rows, gain_pre, gain_post, weight_set):
    gate_full, up_full, down_full = weight_set
    normed = rms_rows(rows, gain_pre)

    def activate(tokens_part, first_row):
        gate_sum = jnp.dot(tokens_part, gate_full, preferred_element_type=jnp.float32)
        up_sum = jnp.dot(tokens_part, up_full, preferred_element_type=jnp.float32)
        return (jax.nn.silu(gate_sum) * up_sum).astype(jnp.bfloat16)

    hidden = on_whole(normed, "tp", 0, activate)

    def project(first_row, row_count):
        row_block = lax.dynamic_slice_in_dim(hidden, first_row, row_count, 0)
        return jnp.dot(row_block, down_full, preferred_element_type=jnp.float32)

    branch = own_rows(project, normed.shape[0], "tp").astype(jnp.bfloat16)
    return add_branch(rows, rms_rows(branch, gain_post), half_weight)


def body(
    stream,
    mixer_out,
    ffn_gains,
    mixer_gain,
    gate_first,
    up_first,
    down_first,
    gate_second,
    up_second,
    down_second,
):
    first_set = collect_weights(gate_first, up_first, down_first)
    after_first = half_step(stream, ffn_gains[0], ffn_gains[1], first_set)
    mixed_in = add_branch(after_first, rms_rows(mixer_out, mixer_gain), 1.0)
    second_set = collect_weights(gate_second, up_second, down_second)
    return half_step(mixed_in, ffn_gains[2], ffn_gains[3], second_set)


def solution(mesh):
    placed = (
        P(("fs", "tp"), None),
        P(("fs", "tp"), None),
        P(),
        P(),
        P("fs", "tp"),
        P("fs", "tp"),
        P("tp", "fs"),
        P("fs", "tp"),
        P("fs", "tp"),
        P("tp", "fs"),
    )
    return jax.shard_map(
        body, mesh=mesh, in_specs=placed, out_specs=P(("fs", "tp"), None), check_vma=False
    )
```

profile of v0, /device:TPU:0, one launch (start us, length us, event | category | flops | bytes accessed | tf_op | source)
XLA Modules:
  0.0 245.0 jit_solution(8046702978109701361)
XLA Ops:
  6.5 0.0 copy-start.6
  6.5 0.0 copy-start.7
  6.5 0.0 copy-start.4
  6.5 0.0 all-gather.11.cloned.1.call-start
  6.5 0.9 reshape.53
  7.5 0.9 reshape.54
  8.4 0.6 pad_maximum_fusion
  9.1 0.0 all-gather.11.cloned.1.call-update
  9.1 0.0 all-gather.7.cloned.1.call-start
  9.1 1.1 fusion.13
  10.2 0.9 fusion.25
  11.1 1.8 fusion.15
  12.9 0.0 all-gather.7.cloned.1.call-update
  12.9 0.0 all-gather.13.cloned.1.call-start
  13.0 0.0 copy-done.6
  13.0 0.1 reshape.55
  13.1 0.0 copy-done.7
  13.1 0.1 reshape.56
  13.3 0.6 pad_maximum_fusion.1
  13.9 0.0 all-gather.13.cloned.1.call-update
  13.9 0.0 reduce-scatter.3.cloned.1.call-start
  14.0 0.0 copy-done.4
  14.0 28.4 %all_gather.27 = bf16[352,1024]{0,1:T(8,128)(2,1)} all-gather(bf16[352,64]{0,1:T(8,128)(2,1)S(1)} %copy-done.4), channel_id=1, replica_groups=mesh['fs'=16,'tp'=8] {'fs'}, dimensions={1}, use_global_device_ids=true | all-gather | bytes 765952 | tf_op jit(solution)/shard_map/all_gather | solution.py:50
  42.4 13.6 %all-gather.11.cloned.1.call-done = bf16[720896]{0:T(1024)(128)(2,1)} async-done(((bf16[45056]{0:T(1024)(128)(2,1)}), bf16[720896]{0:T(1024)(128)(2,1)}) %all-gather.11.cloned.1.call-update) | async-done | bytes 1441808 | tf_op jit(solution)/shard_map/all_gather | solution.py:18
  56.1 1.7 reshape.57
  57.8 0.1 fusion.24
  57.9 1.2 reshape_reshape.12
  59.1 1.2 reshape_reshape.13
  60.3 0.0 copy-start.3
  60.3 22.0 %all-gather.7.cloned.1.call-done = bf16[1024,1024]{1,0:T(8,128)(2,1)} async-done(((bf16[128,1024]{1,0:T(8,128)(2,1)}), bf16[1024,1024]{1,0:T(8,128)(2,1)}) %all-gather.7.cloned.1.call-update) | async-done | bytes 2097168 | tf_op jit(solution)/shard_map/all_gather | solution.py:27
  82.3 3.7 %fusion.26 = f32[1024,352]{0,1:T(8,128)} fusion(bf16[1024,1024]{1,0:T(8,128)(2,1)} %all-gather.7.cloned.1.call-done, bf16[1024,352]{1,0:T(8,128)(2,1)S(1)} %reshape_reshape.12), kind=kOutput, calls=%fused_computation.50 | convolution fusion | flops 738197504 | bytes 4259840 | tf_op jit(solution)/shard_map/dot_general | solution.py:59
  86.0 0.0 copy-done.3
  86.0 5.6 %convolution_convert_fusion.1 = bf16[1024,1024]{1,0:T(8,128)(2,1)} fusion(bf16[352,1024]{0,1:T(8,128)(2,1)S(1)} %copy-done.3, bf16[1024,1024]{1,0:T(8,128)(2,1)} %all-gather.7.cloned.1.call-done, bf16[1024,352]{1,0:T(8,128)(2,1)S(1)} %reshape_reshape.13, f32[1024,352]{0,1:T(8,128)} %fusion.26), kind=kOutput, calls=%fused_computation.1 | convolution fusion | flops 1479606272 | bytes 7077888 | tf_op jit(solution)/shard_map/dot_general | solution.py:67
  91.6 0.0 copy-start.1
  91.6 0.0 reduce-scatter.3.cloned.1.call-update
  91.6 0.0 all-gather.9.cloned.1.call-start
  91.6 0.9 copy-done.1
  92.5 0.1 fusion.7
  92.6 0.0 copy-done.5
  92.7 27.5 %all_gather.31 = bf16[352,1024]{0,1:T(8,128)(2,1)} all-gather(bf16[352,64]{0,1:T(8,128)(2,1)S(1)} %copy-done.5), channel_id=1, replica_groups=mesh['fs'=16,'tp'=8] {'fs'}, dimensions={1}, use_global_device_ids=true | all-gather | bytes 765952 | tf_op jit(solution)/shard_map/all_gather | solution.py:50
  120.1 0.0 copy-start
  120.2 0.0 copy-start.8
  120.2 8.8 %all-gather.13.cloned.1.call-done = bf16[720896]{0:T(1024)(128)(2,1)} async-done(((bf16[45056]{0:T(1024)(128)(2,1)}), bf16[720896]{0:T(1024)(128)(2,1)}) %all-gather.13.cloned.1.call-update) | async-done | bytes 1441808 | tf_op jit(solution)/shard_map/all_gather | solution.py:18
  129.0 1.7 reshape.58
  130.7 33.2 %reduce-scatter.3.cloned.1.call-done = bf16[128,1024]{1,0:T(8,128)(2,1)} async-done(((bf16[1024,1024]{1,0:T(8,128)(2,1)}), bf16[128,1024]{1,0:T(8,128)(2,1)}) %reduce-scatter.3.cloned.1.call-update) | async-done | bytes 262160 | tf_op jit(solution)/shard_map/reduce_scatter | solution.py:33
  163.9 1.1 fusion.4
  165.0 0.0 copy-done
  165.0 0.0 copy-done.8
  165.0 1.3 fusion.17
  166.4 0.8 fusion.19
  167.2 0.0 all-gather.9.cloned.1.call-update
  167.2 0.2 reduce-scatter.5.cloned.1.call-start
  167.4 0.1 fusion.23
  167.6 2.1 reshape_reshape.14
  169.6 1.2 reshape_reshape.15
  170.8 0.0 copy-start.2
  170.8 20.5 %all-gather.9.cloned.1.call-done = bf16[1024,1024]{1,0:T(8,128)(2,1)} async-done(((bf16[128,1024]{1,0:T(8,128)(2,1)}), bf16[1024,1024]{1,0:T(8,128)(2,1)}) %all-gather.9.cloned.1.call-update) | async-done | bytes 2097168 | tf_op jit(solution)/shard_map/all_gather | solution.py:27
  191.4 3.9 %fusion.27 = f32[1024,352]{0,1:T(8,128)} fusion(bf16[1024,1024]{1,0:T(8,128)(2,1)} %all-gather.9.cloned.1.call-done, bf16[1024,352]{1,0:T(8,128)(2,1)} %reshape_reshape.14), kind=kOutput, calls=%fused_computation.51 | convolution fusion | flops 738197504 | bytes 4259840 | tf_op jit(solution)/shard_map/dot_general | solution.py:59
  195.3 0.0 copy-done.2
  195.3 5.6 %convolution_convert_fusion = bf16[1024,1024]{1,0:T(8,128)(2,1)} fusion(bf16[352,1024]{0,1:T(8,128)(2,1)S(1)} %copy-done.2, bf16[1024,1024]{1,0:T(8,128)(2,1)} %all-gather.9.cloned.1.call-done, bf16[1024,352]{1,0:T(8,128)(2,1)S(1)} %reshape_reshape.15, f32[1024,352]{0,1:T(8,128)} %fusion.27), kind=kOutput, calls=%fused_computation | convolution fusion | flops 1479606272 | bytes 7077888 | tf_op jit(solution)/shard_map/dot_general | solution.py:67
  200.9 0.0 reduce-scatter.5.cloned.1.call-update
  200.9 34.4 %reduce-scatter.5.cloned.1.call-done = bf16[128,1024]{1,0:T(8,128)(2,1)} async-done(((bf16[1024,1024]{1,0:T(8,128)(2,1)}), bf16[128,1024]{1,0:T(8,128)(2,1)}) %reduce-scatter.5.cloned.1.call-update) | async-done | bytes 262160 | tf_op jit(solution)/shard_map/reduce_scatter | solution.py:33
  235.2 1.1 fusion.10
  236.3 1.8 fusion.20
  (6 shorter events, 0.0 us)
Async XLA Ops:
  6.5 6.5 %copy-start.6 = (bf16[64,352]{1,0:T(8,128)(2,1)S(1)}, bf16[64,352]{1,0:T(8,128)(2,1)}, u32[]{:S(2)}) copy-start(bf16[64,352]{1,0:T(8,128)(2,1)} %param.17) | copy-start | bytes 135172
  6.5 6.6 %copy-start.7 = (bf16[64,352]{1,0:T(8,128)(2,1)S(1)}, bf16[64,352]{1,0:T(8,128)(2,1)}, u32[]{:S(2)}) copy-start(bf16[64,352]{1,0:T(8,128)(2,1)} %param.18) | copy-start | bytes 135172
  6.5 7.5 %copy-start.4 = (bf16[352,64]{0,1:T(8,128)(2,1)S(1)}, bf16[352,64]{0,1:T(8,128)(2,1)}, u32[]{:S(2)}) copy-start(bf16[352,64]{0,1:T(8,128)(2,1)} %param.16) | copy-start | bytes 135172
  6.5 49.5 %all-gather.11.cloned.1.call-start = ((), (), s32[]{:S(2)}) async-start(), calls=%async_computation.6 | async-start | bytes 1531904 | tf_op jit(solution)/shard_map/all_gather | solution.py:18
  9.1 73.2 %all-gather.7.cloned.1.call-start = ((), (), s32[]{:S(2)}) async-start(), calls=%async_computation.2 | async-start | bytes 2359296 | tf_op jit(solution)/shard_map/all_gather | solution.py:27
  12.9 116.0 %all-gather.13.cloned.1.call-start = ((), (), s32[]{:S(2)}) async-start(), calls=%async_computation.7 | async-start | bytes 1531904 | tf_op jit(solution)/shard_map/all_gather | solution.py:18
  13.9 150.0 %reduce-scatter.3.cloned.1.call-start = ((), (), s32[]{:S(2)}) async-start(), calls=%async_computation.3 | async-start | bytes 2359296 | tf_op jit(solution)/shard_map/reduce_scatter | solution.py:33
  60.3 25.7 %copy-start.3 = (bf16[352,1024]{0,1:T(8,128)(2,1)S(1)}, bf16[352,1024]{0,1:T(8,128)(2,1)}, u32[]{:S(2)}) copy-start(bf16[352,1024]{0,1:T(8,128)(2,1)} %all_gather.27) | copy-start | bytes 2162692
  91.6 0.9 copy-start.1
  91.6 1.1 copy-start.5
  91.6 99.8 %all-gather.9.cloned.1.call-start = ((), (), s32[]{:S(2)}) async-start(), calls=%async_computation.4 | async-start | bytes 2359296 | tf_op jit(solution)/shard_map/all_gather | solution.py:27
  120.1 44.8 %copy-start = (bf16[128,1024]{1,0:T(8,128)(2,1)S(1)}, bf16[128,1024]{1,0:T(8,128)(2,1)}, u32[]{:S(2)}) copy-start(bf16[128,1024]{1,0:T(8,128)(2,1)} %param.10) | copy-start | bytes 786436
  120.2 44.8 %copy-start.8 = (f32[1024]{0:T(1024)S(1)}, f32[1024]{0:T(1024)}, u32[]{:S(2)}) copy-start(f32[1024]{0:T(1024)} %param.13) | copy-start | bytes 12292
  167.2 68.0 %reduce-scatter.5.cloned.1.call-start = ((), (), s32[]{:S(2)}) async-start(), calls=%async_computation.5 | async-start | bytes 2359296 | tf_op jit(solution)/shard_map/reduce_scatter | solution.py:33
  170.8 24.4 %copy-start.2 = (bf16[352,1024]{0,1:T(8,128)(2,1)S(1)}, bf16[352,1024]{0,1:T(8,128)(2,1)}, u32[]{:S(2)}) copy-start(bf16[352,1024]{0,1:T(8,128)(2,1)} %all_gather.31) | copy-start | bytes 2162692
Sparse Core Ops, SparseCore 0:
  9.5 46.5 all-gather.10
  57.8 24.4 all-gather.6
  84.4 44.4 all-gather.12
  131.2 32.6 reduce-scatter.2
  167.3 23.9 all-gather.8
  201.0 34.1 reduce-scatter.4
where the time goes:
time: 246 us; the launch traced here: 245 us
  waiting for transfers between devices  133 us (54%)
  blocking collectives  55.9 us (23%)
  matrix products  18.7 us (8%)
  between operations  13.6 us (6%)
  local copies, waits for them, and re-layouts  13.3 us (5%)
  other arithmetic  10.5 us (4%)
    reduce_scatter x2, waiting for transfers between devices, own_rows(): lax.psum_scatter(sent, axis, scatter_dimension=0, tiled=True)  67.5 us
    all_gather x2, blocking collectives, collect_weights(): down_full = lax.all_gather(down_local, 'fs', axis=1, tiled=True)  55.9 us
    all_gather x2, waiting for transfers between devices, on_whole(): return work(lax.all_gather(shard, axis, axis=dim, tiled=True), jnp.int32(0))  42.5 us
    all_gather x2, waiting for transfers between devices, gather_together(): lines, at, gathered = (lax.all_gather(line, axis), 0, [])  22.4 us
    dot_general x2, matrix products, project(): return jnp.dot(row_block, down_full, preferred_element_type=jnp.float32)  11.2 us
    dot_general x2, matrix products, activate(): jnp.dot(tokens_part, gate_full, preferred_element_type=jnp.float32)  7.55 us
    another operation x4, local copies, waits for them, and re-layouts, laid_out(): return jnp.moveaxis(blocks, 0, dim).reshape(dims)  5.66 us
  transfers between devices with their start and end apart: 6, of which 6 were waited for; matrix products, arithmetic and copies ran while one was open for 10% of the time, Pallas kernels for 0%

commit v1 on v0

--- a/solution.py
+++ b/solution.py
@@ -5,6 +5,13 @@
 
 epsilon = 1e-06
 half_weight = 0.5
+
+
+def swapped_in(x, axis, dim):
+    size = lax.axis_size(axis)
+    tiles = jnp.stack([x for _ in range(size)])
+    tiles = lax.all_to_all(tiles, axis, split_axis=0, concat_axis=0)
+    return jnp.concatenate(tiles, axis=dim)
 
 
 def laid_out(blocks, dim):
@@ -47,7 +54,7 @@
 
 def collect_weights(gate_local, up_local, down_local):
     gate_full, up_full = gather_together((gate_local, up_local), "fs", (0, 0))
-    down_full = lax.all_gather(down_local, "fs", axis=1, tiled=True)
+    down_full = swapped_in(down_local, "fs", 1)
     return (gate_full, up_full, down_full)
 
 

time: 246 us -> 256 us (1.041)
  blocking collectives: 55.9 us -> 0 us
  waiting for transfers between devices: 133 us -> 181 us
  starting transfers between devices: 0.39 us -> 15.6 us
    all_gather x2 -> x0, blocking collectives: 55.9 us -> none  [collect_weights(): down_full = lax.all_gather(down_local, 'fs', axis=1, tiled=True)]
    all_gather x2, waiting for transfers between devices: 22.4 us -> 70.3 us  [gather_together(): lines, at, gathered = (lax.all_gather(line, axis), 0, [])]
    all_to_all x0 -> x2, starting transfers between devices: none -> 15.2 us  [swapped_in(): tiles = lax.all_to_all(tiles, axis, split_axis=0, concat_axis=0)]
  transfers between devices with their start and end apart: 6 -> 8, of which waited for: 6 -> 6; matrix products, arithmetic and copies ran while one was open for 10% -> 13% of each run, Pallas kernels for 0% -> 0%
where the time goes in v1:
time: 256 us; the launch traced here: 255 us
  waiting for transfers between devices  181 us (71%)
  matrix products  19 us (7%)
  starting transfers between devices  15.6 us (6%)
  local copies, waits for them, and re-layouts  15.3 us (6%)
  between operations  13.6 us (5%)
  other arithmetic  10.5 us (4%)
    all_gather x2, waiting for transfers between devices, gather_together(): lines, at, gathered = (lax.all_gather(line, axis), 0, [])  70.3 us
    reduce_scatter x2, waiting for transfers between devices, own_rows(): lax.psum_scatter(sent, axis, scatter_dimension=0, tiled=True)  68 us
    all_gather x2, waiting for transfers between devices, on_whole(): return work(lax.all_gather(shard, axis, axis=dim, tiled=True), jnp.int32(0))  42.6 us
    all_to_all x2, starting transfers between devices, swapped_in(): tiles = lax.all_to_all(tiles, axis, split_axis=0, concat_axis=0)  15.2 us
    dot_general x2, matrix products, project(): return jnp.dot(row_block, down_full, preferred_element_type=jnp.float32)  11.6 us
    dot_general x2, matrix products, activate(): jnp.dot(tokens_part, gate_full, preferred_element_type=jnp.float32)  7.39 us
    another operation x4, local copies, waits for them, and re-layouts, laid_out(): return jnp.moveaxis(blocks, 0, dim).reshape(dims)  5.67 us
  transfers between devices with their start and end apart: 8, of which 6 were waited for; matrix products, arithmetic and copies ran while one was open for 13% of the time, Pallas kernels for 0%

profile of v1, /device:TPU:0, one launch (start us, length us, event | category | flops | bytes accessed | tf_op | source)
XLA Modules:
  0.0 255.0 jit_solution(15520524956206022996)
XLA Ops:
  6.5 0.0 copy-start.3
  6.5 0.0 all-gather.11.cloned.1.call-start
  6.5 0.9 reshape.69
  7.5 0.9 reshape.70
  8.4 0.6 pad_maximum_fusion
  9.1 0.0 all-gather.11.cloned.1.call-update
  9.1 0.0 all-gather.7.cloned.1.call-start
  9.1 1.1 fusion.13
  10.2 0.9 fusion.25
  11.1 1.8 fusion.15
  12.9 0.0 copy-start.5
  12.9 0.0 all-gather.7.cloned.1.call-update
  12.9 0.0 copy-done.3
  12.9 1.1 stack.4
  14.0 8.2 %all-to-all-start = ((bf16[16,352,64]{1,2,0:T(8,128)(2,1)}), bf16[16,352,64]{1,2,0:T(8,128)(2,1)}, u32[]{:S(2)}, u32[]{:S(2)}) async-start(bf16[16,352,64]{1,2,0:T(8,128)(2,1)} %stack.4), calls=%async_computation | async-start | bytes 1572864 | tf_op jit(solution)/shard_map/all_to_all | solution.py:13
  22.2 0.0 all-gather.13.cloned.1.call-start
  22.3 0.0 copy-done.5
  22.3 0.1 reshape.73
  22.4 0.0 copy-done.6
  22.4 0.1 reshape.74
  22.6 0.6 pad_maximum_fusion.1
  23.2 0.0 all-gather.13.cloned.1.call-update
  23.2 0.0 reduce-scatter.3.cloned.1.call-start
  23.3 37.1 %all-gather.11.cloned.1.call-done = bf16[720896]{0:T(1024)(128)(2,1)} async-done(((bf16[45056]{0:T(1024)(128)(2,1)}), bf16[720896]{0:T(1024)(128)(2,1)}) %all-gather.11.cloned.1.call-update) | async-done | bytes 1441808 | tf_op jit(solution)/shard_map/all_gather | solution.py:25
  60.4 1.7 reshape.77
  62.1 0.1 fusion.24
  62.2 1.2 reshape_reshape.12
  63.4 1.2 reshape_reshape.13
  64.6 22.0 %all-gather.7.cloned.1.call-done = bf16[1024,1024]{1,0:T(8,128)(2,1)} async-done(((bf16[128,1024]{1,0:T(8,128)(2,1)}), bf16[1024,1024]{1,0:T(8,128)(2,1)}) %all-gather.7.cloned.1.call-update) | async-done | bytes 2097168 | tf_op jit(solution)/shard_map/all_gather | solution.py:34
  86.6 3.7 %fusion.26 = f32[1024,352]{0,1:T(8,128)} fusion(bf16[1024,1024]{1,0:T(8,128)(2,1)} %all-gather.7.cloned.1.call-done, bf16[1024,352]{1,0:T(8,128)(2,1)S(1)} %reshape_reshape.12), kind=kOutput, calls=%fused_computation.50 | convolution fusion | flops 738197504 | bytes 4259840 | tf_op jit(solution)/shard_map/dot_general | solution.py:66
  90.3 0.0 all-to-all-done
  90.3 5.8 %convolution_convert_fusion.1 = bf16[1024,1024]{1,0:T(8,128)(2,1)} fusion(bf16[352,1024]{0,1:T(8,128)(2,1)} %bitcast.2, bf16[1024,1024]{1,0:T(8,128)(2,1)} %all-gather.7.cloned.1.call-done, bf16[1024,352]{1,0:T(8,128)(2,1)S(1)} %reshape_reshape.13, f32[1024,352]{0,1:T(8,128)} %fusion.26), kind=kOutput, calls=%fused_computation.1 | convolution fusion | flops 1479606272 | bytes 7077888 | tf_op jit(solution)/shard_map/dot_general | solution.py:74
  96.1 0.0 copy-start.4
  96.1 0.0 reduce-scatter.3.cloned.1.call-update
  96.1 0.8 copy-done.4
  96.9 0.0 copy-start.1
  96.9 1.0 stack.5
  97.9 7.0 %all-to-all-start.1 = ((bf16[16,352,64]{1,2,0:T(8,128)(2,1)}), bf16[16,352,64]{1,2,0:T(8,128)(2,1)}, u32[]{:S(2)}, u32[]{:S(2)}) async-start(bf16[16,352,64]{1,2,0:T(8,128)(2,1)} %stack.5), calls=%async_computation.2 | async-start | bytes 1572864 | tf_op jit(solution)/shard_map/all_to_all | solution.py:13
  104.9 0.0 all-gather.9.cloned.1.call-start
  105.0 0.0 copy-done.1
  105.0 0.1 fusion.7
  105.2 0.0 copy-start.7
  105.2 33.2 %all-gather.13.cloned.1.call-done = bf16[720896]{0:T(1024)(128)(2,1)} async-done(((bf16[45056]{0:T(1024)(128)(2,1)}), bf16[720896]{0:T(1024)(128)(2,1)}) %all-gather.13.cloned.1.call-update) | async-done | bytes 1441808 | tf_op jit(solution)/shard_map/all_gather | solution.py:25
  138.4 1.7 reshape.78
  140.1 33.6 %reduce-scatter.3.cloned.1.call-done = bf16[128,1024]{1,0:T(8,128)(2,1)} async-done(((bf16[1024,1024]{1,0:T(8,128)(2,1)}), bf16[128,1024]{1,0:T(8,128)(2,1)}) %reduce-scatter.3.cloned.1.call-update) | async-done | bytes 262160 | tf_op jit(solution)/shard_map/reduce_scatter | solution.py:40
  173.8 1.1 fusion.4
  174.9 0.0 copy-done
  174.9 0.0 copy-done.7
  174.9 1.3 fusion.17
  176.2 0.8 fusion.19
  177.1 0.0 all-gather.9.cloned.1.call-update
  177.1 0.2 reduce-scatter.5.cloned.1.call-start
  177.3 0.1 fusion.23
  177.4 2.1 reshape_reshape.14
  179.5 1.2 reshape_reshape.15
  180.7 20.6 %all-gather.9.cloned.1.call-done = bf16[1024,1024]{1,0:T(8,128)(2,1)} async-done(((bf16[128,1024]{1,0:T(8,128)(2,1)}), bf16[1024,1024]{1,0:T(8,128)(2,1)}) %all-gather.9.cloned.1.call-update) | async-done | bytes 2097168 | tf_op jit(solution)/shard_map/all_gather | solution.py:34
  201.3 0.0 copy-done.2
  201.3 3.7 %fusion.27 = f32[1024,352]{0,1:T(8,128)} fusion(bf16[1024,1024]{1,0:T(8,128)(2,1)} %all-gather.9.cloned.1.call-done, bf16[1024,352]{1,0:T(8,128)(2,1)S(1)} %copy-done.2), kind=kOutput, calls=%fused_computation.51 | convolution fusion | flops 738197504 | bytes 4259840 | tf_op jit(solution)/shard_map/dot_general | solution.py:66
  205.0 0.0 all-to-all-done.1
  205.0 5.8 %convolution_convert_fusion = bf16[1024,1024]{1,0:T(8,128)(2,1)} fusion(bf16[352,1024]{0,1:T(8,128)(2,1)} %bitcast.6, bf16[1024,1024]{1,0:T(8,128)(2,1)} %all-gather.9.cloned.1.call-done, bf16[1024,352]{1,0:T(8,128)(2,1)S(1)} %reshape_reshape.15, f32[1024,352]{0,1:T(8,128)} %fusion.27), kind=kOutput, calls=%fused_computation | convolution fusion | flops 1479606272 | bytes 7077888 | tf_op jit(solution)/shard_map/dot_general | solution.py:74
  210.8 0.0 reduce-scatter.5.cloned.1.call-update
  210.8 34.4 %reduce-scatter.5.cloned.1.call-done = bf16[128,1024]{1,0:T(8,128)(2,1)} async-done(((bf16[1024,1024]{1,0:T(8,128)(2,1)}), bf16[128,1024]{1,0:T(8,128)(2,1)}) %reduce-scatter.5.cloned.1.call-update) | async-done | bytes 262160 | tf_op jit(solution)/shard_map/reduce_scatter | solution.py:40
  245.2 1.1 fusion.10
  246.3 1.8 fusion.20
  (8 shorter events, 0.0 us)
Async XLA Ops:
  6.5 6.4 %copy-start.3 = (bf16[352,64]{0,1:T(8,128)(2,1)S(1)}, bf16[352,64]{0,1:T(8,128)(2,1)}, u32[]{:S(2)}) copy-start(bf16[352,64]{0,1:T(8,128)(2,1)} %param.16) | copy-start | bytes 135172
  6.5 53.8 %all-gather.11.cloned.1.call-start = ((), (), s32[]{:S(2)}) async-start(), calls=%async_computation.8 | async-start | bytes 1531904 | tf_op jit(solution)/shard_map/all_gather | solution.py:25
  9.1 77.5 %all-gather.7.cloned.1.call-start = ((), (), s32[]{:S(2)}) async-start(), calls=%async_computation.4 | async-start | bytes 2359296 | tf_op jit(solution)/shard_map/all_gather | solution.py:34
  12.9 9.4 %copy-start.5 = (bf16[64,352]{1,0:T(8,128)(2,1)S(1)}, bf16[64,352]{1,0:T(8,128)(2,1)}, u32[]{:S(2)}) copy-start(bf16[64,352]{1,0:T(8,128)(2,1)} %param.17) | copy-start | bytes 135172
  12.9 9.5 %copy-start.6 = (bf16[64,352]{1,0:T(8,128)(2,1)S(1)}, bf16[64,352]{1,0:T(8,128)(2,1)}, u32[]{:S(2)}) copy-start(bf16[64,352]{1,0:T(8,128)(2,1)} %param.18) | copy-start | bytes 135172
  14.0 76.3 %all-to-all-start = ((bf16[16,352,64]{1,2,0:T(8,128)(2,1)}), bf16[16,352,64]{1,2,0:T(8,128)(2,1)}, u32[]{:S(2)}, u32[]{:S(2)}) async-start(bf16[16,352,64]{1,2,0:T(8,128)(2,1)} %stack.4), calls=%async_computation | async-start | bytes 1572864 | tf_op jit(solution)/shard_map/all_to_all | solution.py:13
  22.2 116.2 %all-gather.13.cloned.1.call-start = ((), (), s32[]{:S(2)}) async-start(), calls=%async_computation.9 | async-start | bytes 1531904 | tf_op jit(solution)/shard_map/all_gather | solution.py:25
  23.2 150.5 %reduce-scatter.3.cloned.1.call-start = ((), (), s32[]{:S(2)}) async-start(), calls=%async_computation.5 | async-start | bytes 2359296 | tf_op jit(solution)/shard_map/reduce_scatter | solution.py:40
  96.1 0.8 copy-start.4
  96.9 8.1 %copy-start.1 = (bf16[128,1024]{1,0:T(8,128)(2,1)S(1)}, bf16[128,1024]{1,0:T(8,128)(2,1)}, u32[]{:S(2)}) copy-start(bf16[128,1024]{1,0:T(8,128)(2,1)} %param.11) | copy-start | bytes 786436
  97.9 107.1 %all-to-all-start.1 = ((bf16[16,352,64]{1,2,0:T(8,128)(2,1)}), bf16[16,352,64]{1,2,0:T(8,128)(2,1)}, u32[]{:S(2)}, u32[]{:S(2)}) async-start(bf16[16,352,64]{1,2,0:T(8,128)(2,1)} %stack.5), calls=%async_computation.2 | async-start | bytes 1572864 | tf_op jit(solution)/shard_map/all_to_all | solution.py:13
  104.9 96.3 %all-gather.9.cloned.1.call-start = ((), (), s32[]{:S(2)}) async-start(), calls=%async_computation.6 | async-start | bytes 2359296 | tf_op jit(solution)/shard_map/all_gather | solution.py:34
  105.1 69.7 %copy-start = (bf16[128,1024]{1,0:T(8,128)(2,1)S(1)}, bf16[128,1024]{1,0:T(8,128)(2,1)}, u32[]{:S(2)}) copy-start(bf16[128,1024]{1,0:T(8,128)(2,1)} %param.10) | copy-start | bytes 786436
  105.2 69.7 %copy-start.7 = (f32[1024]{0:T(1024)S(1)}, f32[1024]{0:T(1024)}, u32[]{:S(2)}) copy-start(f32[1024]{0:T(1024)} %param.13) | copy-start | bytes 12292
  177.1 68.1 %reduce-scatter.5.cloned.1.call-start = ((), (), s32[]{:S(2)}) async-start(), calls=%async_computation.7 | async-start | bytes 2359296 | tf_op jit(solution)/shard_map/reduce_scatter | solution.py:40
  179.5 21.8 %copy-start.2 = (bf16[1024,352]{1,0:T(8,128)(2,1)S(1)}, bf16[1024,352]{1,0:T(8,128)(2,1)}, u32[]{:S(2)}) copy-start(bf16[1024,352]{1,0:T(8,128)(2,1)} %reshape_reshape.14) | copy-start | bytes 2162692
Sparse Core Ops, SparseCore 0:
  9.5 50.8 all-gather.10
  62.1 24.4 all-gather.6
  88.8 49.5 all-gather.12
  140.6 33.0 reduce-scatter.2
  177.2 24.0 all-gather.8
  210.9 34.2 reduce-scatter.4
